TPU v7x, 32 devices: a whole 2x2x4 slice. The times are simulated.
32 devices in a mesh: sp: 16 (over z, y, x), tp: 2 (over core).
Axes of the slice: x: 2, y: 2, z: 4, core: 2. Of those that a mesh axis runs over, the one named last changes fastest.
Arguments:
- latent: bfloat16 [4096, 2048], P(('sp', 'tp')), may hold values from -6 to 6
- cond: float32 [2048], replicated, may hold values from -6 to 6
- ctx_mod: float32 [2048], replicated, may hold values from -6 to 6
- context: bfloat16 [512, 2048], P(('sp', 'tp')), may hold values from -6 to 6
- shift_w: float32 [2048, 2048], P('sp', 'tp'), may hold values from -0.125 to 0.125
- scale_w: float32 [2048, 2048], P('sp', 'tp'), may hold values from -0.125 to 0.125
- gate_w: float32 [2048, 2048], P('sp', 'tp'), may hold values from -0.125 to 0.125
- norm_gain: float32 [2048], replicated, may hold values from 0.1 to 1.9
- w_qn: bfloat16 [2048, 2048], P(None, 'tp'), may hold values from -0.125 to 0.125
- w_qr: bfloat16 [2048, 1024], P(None, 'tp'), may hold values from -0.13258252 to 0.13258252
- w_kv_down: bfloat16 [2048, 512], replicated, may hold values from -0.125 to 0.125
- w_rope_key: bfloat16 [2048, 64], replicated, may hold values from -0.13258252 to 0.13258252
- kv_gain: float32 [512], replicated, may hold values from 0.1 to 1.9
- w_key_up: bfloat16 [512, 2048], P(None, 'tp'), may hold values from -0.66015625 to 0.66015625
- w_value_up: bfloat16 [512, 2048], P(None, 'tp'), may hold values from -0.25 to 0.25
- ctx_bias: float32 [16], P('tp'), may hold values from 2 to 3.5
- w_out: bfloat16 [2048, 2048], P('tp'), may hold values from -0.52734375 to 0.52734375
Outputs:
- mixed: bfloat16 [4096, 2048], P(('sp', 'tp'))
All inputs are finite; a program needn't handle non-finite values.
Results may differ from a plain program's by a relative error of at most 0.018.
Values may be sent and summed in bfloat16 or wider, within the bound.
A program may use at most 128 MiB of HBM per device.

v0:
```python
import jax
import jax.numpy as jnp
from jax import lax
from jax.sharding import PartitionSpec as P

GRID_W = 128


EPS = 1e-06
ROPE_BASE = 10000.0


def modulate(rows_in, gain, shift, scale):
    values = rows_in.astype(jnp.float32)
    normed = values * lax.rsqrt(jnp.mean(values * values, axis=-1, keepdims=True) + EPS)
    return (normed * gain * (1.0 + scale) + shift).astype(jnp.bfloat16)


def compress(rows_in, w_kv_down, kv_gain):
    inner = jnp.dot(rows_in, w_kv_down, preferred_element_type=jnp.float32)
    normed = inner * lax.rsqrt(jnp.mean(inner * inner, axis=-1, keepdims=True) + EPS)
    return (normed * kv_gain).astype(jnp.bfloat16)


def angles(positions, rope_dim):
    quarter = rope_dim // 4
    inverse = ROPE_BASE ** (-jnp.arange(quarter, dtype=jnp.float32) / quarter)
    row = (positions // GRID_W).astype(jnp.float32)
    column = (positions % GRID_W).astype(jnp.float32)
    return jnp.concatenate(
        [row[:, None] * inverse[None, :], column[:, None] * inverse[None, :]], axis=-1
    )


def rotate(values, angle):
    pairs = values.reshape(values.shape[:-1] + (values.shape[-1] // 2, 2))
    first = pairs[..., 0]
    second = pairs[..., 1]
    cosine = jnp.cos(angle)
    sine = jnp.sin(angle)
    turned = jnp.stack([first * cosine - second * sine, first * sine + second * cosine], axis=-1)
    return turned.reshape(values.shape)


def body(
    latent,
    cond,
    ctx_mod,
    context,
    shift_w,
    scale_w,
    gate_w,
    norm_gain,
    w_qn,
    w_qr,
    w_kv_down,
    w_rope_key,
    kv_gain,
    w_key_up,
    w_value_up,
    ctx_bias,
    w_out,
):
    n_tp = lax.axis_size("tp")
    sp_index = lax.axis_index("sp")
    tp_index = lax.axis_index("tp")
    rows = latent.shape[0]
    ctx_rows = context.shape[0]
    width = latent.shape[1]
    tok_dev = rows * n_tp
    heads_dev = ctx_bias.shape[0]
    nope = w_key_up.shape[1] // heads_dev
    vsize = w_value_up.shape[1] // heads_dev
    rope = w_rope_key.shape[1]
    period = rows + ctx_rows
    factor = (nope + rope) ** (-0.5)
    pair = jnp.stack([jax.nn.silu(cond), jax.nn.silu(ctx_mod)])
    feat_block = shift_w.shape[0]
    pair_block = lax.dynamic_slice_in_dim(pair, sp_index * feat_block, feat_block, 1)
    partials = tuple(
        (
            jnp.dot(pair_block, weight, precision=lax.Precision.HIGHEST)
            for weight in (shift_w, scale_w, gate_w)
        )
    )
    columns = shift_w.shape[1]
    placed = tuple(
        (
            lax.dynamic_update_slice_in_dim(
                jnp.zeros((2, width), jnp.float32), part, tp_index * columns, 1
            )
            for part in partials
        )
    )
    shift, scale, gate = lax.psum((placed[0], placed[1], placed[2]), ("sp", "tp"))
    h_rows = modulate(latent, norm_gain, shift[0], scale[0])
    h_ctx = modulate(context, norm_gain, shift[1], scale[1])
    own_positions = sp_index * tok_dev + tp_index * rows + jnp.arange(rows, dtype=jnp.int32)
    own_latents = jnp.concatenate(
        [compress(h_rows, w_kv_down, kv_gain), compress(h_ctx, w_kv_down, kv_gain)], axis=0
    )
    rope_rows = rotate(
        jnp.dot(h_rows, w_rope_key, preferred_element_type=jnp.float32), angles(own_positions, rope)
    ).astype(jnp.bfloat16)
    rope_ctx = jnp.dot(h_ctx, w_rope_key, preferred_element_type=jnp.float32).astype(jnp.bfloat16)
    own_rope = jnp.concatenate([rope_rows, rope_ctx], axis=0)
    piece = lax.all_gather(h_rows, "tp", axis=0, tiled=True)
    count = piece.shape[0]
    nope_part = jnp.dot(piece, w_qn, preferred_element_type=jnp.float32).astype(jnp.bfloat16)
    places = sp_index * tok_dev + jnp.arange(count, dtype=jnp.int32)
    rope_part = jnp.dot(piece, w_qr, preferred_element_type=jnp.float32).reshape(
        count, heads_dev, rope
    )
    rope_part = rotate(rope_part, angles(places, rope)[:, None, :]).reshape(count, heads_dev * rope)
    queries = jnp.concatenate([nope_part, rope_part.astype(jnp.bfloat16)], axis=1)
    query_nope = queries[:, : heads_dev * nope].reshape(tok_dev, heads_dev, nope)
    query_rope = queries[:, heads_dev * nope :].reshape(tok_dev, heads_dev, rope)

    def fold_keys(carry, keys, values, rope_keys):
        best, total, accum = carry
        count = rope_keys.shape[0]
        keys = keys.reshape(count, heads_dev, nope)
        values = values.reshape(count, heads_dev, vsize)
        scores = jnp.einsum("qhd,khd->hqk", query_nope, keys, preferred_element_type=jnp.float32)
        scores = scores + jnp.einsum(
            "qhr,kr->hqk", query_rope, rope_keys, preferred_element_type=jnp.float32
        )
        index = jnp.arange(count, dtype=jnp.int32)
        is_ctx = (index % period >= rows).astype(jnp.float32)
        scores = scores * factor + ctx_bias[:, None, None] * is_ctx[None, None, :]
        new_best = jnp.maximum(best, jnp.max(scores, axis=-1))
        weights = jnp.exp(scores - new_best[..., None])
        total = jnp.sum(weights, axis=-1)
        accum = jnp.einsum(
            "hqk,khd->hqd", weights.astype(jnp.bfloat16), values, preferred_element_type=jnp.float32
        )
        return (new_best, total, accum)

    start_carry = (
        jnp.full((heads_dev, tok_dev), -1e30, jnp.float32),
        jnp.zeros((heads_dev, tok_dev), jnp.float32),
        jnp.zeros((heads_dev, tok_dev, vsize), jnp.float32),
    )
    pieces = (
        lax.all_gather(own_latents, ("sp", "tp"), axis=0, tiled=True),
        lax.all_gather(own_rope, ("sp", "tp"), axis=0, tiled=True),
    )
    keys = jnp.dot(pieces[0], w_key_up, preferred_element_type=jnp.float32).astype(jnp.bfloat16)
    values = jnp.dot(pieces[0], w_value_up, preferred_element_type=jnp.float32).astype(jnp.bfloat16)
    best, total, accum = fold_keys(start_carry, keys, values, pieces[1])
    attended = (accum / total[..., None]).astype(jnp.bfloat16)
    attended = jnp.transpose(attended, (1, 0, 2)).reshape(tok_dev, heads_dev * vsize)
    part = attended
    branch = lax.psum_scatter(
        jnp.dot(part, w_out, preferred_element_type=jnp.float32).astype(jnp.bfloat16),
        "tp",
        scatter_dimension=0,
        tiled=True,
    ).astype(jnp.float32)
    return (latent.astype(jnp.float32) + gate[0] * branch).astype(jnp.bfloat16)


def solution(mesh):
    placed = (
        P(("sp", "tp"), None),
        P(),
        P(),
        P(("sp", "tp"), None),
        P("sp", "tp"),
        P("sp", "tp"),
        P("sp", "tp"),
        P(),
        P(None, "tp"),
        P(None, "tp"),
        P(),
        P(),
        P(),
        P(None, "tp"),
        P(None, "tp"),
        P("tp"),
        P("tp", None),
    )
    return jax.shard_map(
        body, mesh=mesh, in_specs=placed, out_specs=P(("sp", "tp"), None), check_vma=False
    )
```

profile of v0, /device:TPU:0, one launch (start us, length us, event | category | flops | bytes accessed | tf_op | source)
XLA Modules:
  0.0 253.4 jit_solution(1283834722461088093)
XLA Ops:
  6.6 0.9 divide_multiply_fusion.1
  7.5 0.7 divide_multiply_fusion
  8.2 1.2 fusion.17
  9.4 1.4 convolution_dynamic-update-slice_fusion.1
  10.9 1.4 convolution_dynamic-update-slice_fusion.2
  12.3 1.4 convolution_dynamic-update-slice_fusion
  13.8 42.5 %all-reduce = (f32[2,2048]{1,0:T(2,128)S(1)}, f32[2,2048]{1,0:T(2,128)S(1)}, f32[2,2048]{1,0:T(2,128)S(1)}) all-reduce(f32[2,2048]{1,0:T(2,128)S(1)} %convolution_dynamic-update-slice_fusion, f32[2,2048]{1,0:T(2,128)S(1)} %convolution_dynamic-update-slice_fusion.1, ...), channel_id=1, replica_groups=mesh['sp'=16,'tp'=2] {'sp','tp'}, use_global_device_ids=true, to_apply=%region_3.4 | all-reduce | flops 12288 | bytes 98304 | tf_op jit(solution)/shard_map/psum | solution.py:95
  56.3 2.1 fusion.21
  58.5 2.3 multiply_reduce_fusion
  60.8 1.0 fusion.26
  61.8 2.2 multiply_reduce_fusion.1
  64.0 0.8 multiply_convert_fusion.1
  64.7 0.8 multiply_convert_fusion
  65.5 0.7 pad_maximum_fusion.1
  66.4 1.3 fusion.55
  68.3 44.1 %all-gather = bf16[32,144,64]{1,2,0:T(8,128)(2,1)S(1)} all-gather(bf16[1,144,64]{1,2,0:T(8,128)(2,1)S(1)} %maximum_bitcast_fusion), channel_id=1, replica_groups=mesh['sp'=16,'tp'=2] {'sp','tp'}, dimensions={0}, use_global_device_ids=true | all-gather | bytes 608256 | tf_op jit(solution)/shard_map/all_gather | solution.py:146
  112.4 0.6 copy.50
  113.0 2.5 reshape.383
  115.8 2.5 fusion.56
  118.6 0.7 subtract_convert_fusion
  119.3 0.6 pad_maximum_fusion
  120.0 3.8 %fusion.10 = bf16[32,8,8,128]{3,2,1,0:T(8,128)(2,1)S(1)} fusion(bf16[256,2048]{1,0:T(8,128)(2,1)} %all-gather.4.cloned.1.call-done, bf16[2048,1024]{1,0:T(8,128)(2,1)} %param.25), kind=kOutput, calls=%fused_computation.16 | convolution fusion | flops 1074003968 | bytes 5767168 | tf_op jit(solution)/shard_map/dot_general | solution.py:109
  123.8 12.6 %all-gather.6.cloned.1.call-done = bf16[4608,512]{1,0:T(8,128)(2,1)} async-done(((bf16[144,512]{1,0:T(8,128)(2,1)}), bf16[4608,512]{1,0:T(8,128)(2,1)}) %all-gather.6.cloned.1.call-update) | async-done | bytes 4718608 | tf_op jit(solution)/shard_map/all_gather | solution.py:145
  136.4 9.5 %convolution_convert_fusion.1 = bf16[4608,1024]{0,1:T(8,128)(2,1)} fusion(bf16[4608,512]{1,0:T(8,128)(2,1)} %all-gather.6.cloned.1.call-done, bf16[512,1024]{1,0:T(8,128)(2,1)} %param.30), kind=kOutput, calls=%fused_computation.9 | convolution fusion | flops 4836556800 | bytes 15204352 | tf_op jit(solution)/shard_map/dot_general | solution.py:148
  145.9 18.4 %fusion.23 = f32[8,256,4608]{2,1,0:T(8,128)} fusion(bf16[4608,8,128]{0,2,1:T(8,128)(2,1)} %bitcast.68, bf16[32,8,8,128]{3,2,1,0:T(8,128)(2,1)S(1)} %fusion.10), kind=kOutput, calls=%fused_computation.29 | convolution fusion | flops 2415919104 | bytes 47710208 | tf_op jit(solution)/shard_map/qhd,khd->hqk/dot_general | solution.py:124
  164.3 27.8 %fusion.54 = (f32[8,256]{1,0:T(8,128)S(1)}, f32[8,256,4608]{2,1,0:T(8,128)}) fusion(f32[8,4608]{1,0:T(8,128)S(1)} %broadcast_multiply_fusion, f32[8,256,4608]{2,1,0:T(8,128)} %fusion.23, bf16[4608,64,1]{0,1,2:T(8,128)(2,1)S(1)} %copy-done.3, bf16[256,8,64]{0,2,1:T(8,128)(2,1)S(1)} %convert_element_type.105), kind=kOutput, calls=%fused_computation.103 | convolution fusion | flops 1245706240 | bytes 76505088 | tf_op jit(solution)/shard_map/qhr,kr->hqk/dot_general | solution.py:125
  192.1 16.3 %fusion.2 = f32[8,256]{1,0:T(8,128)S(1)} fusion(f32[8,256,4608]{2,1,0:T(8,128)} %get-tuple-element.29, f32[8,256]{1,0:T(8,128)S(1)} %broadcast_maximum_fusion), kind=kLoop, calls=%fused_computation.4 | loop fusion | flops 18872320 | bytes 37765120 | tf_op jit(solution)/shard_map/reduce_sum | solution.py:133
  208.4 9.9 %convolution_convert_fusion = bf16[4608,1024]{0,1:T(8,128)(2,1)} fusion(bf16[4608,512]{1,0:T(8,128)(2,1)} %all-gather.6.cloned.1.call-done, bf16[512,1024]{1,0:T(8,128)(2,1)S(1)} %copy-done.9), kind=kOutput, calls=%fused_computation.8 | convolution fusion | flops 4836556800 | bytes 15204352 | tf_op jit(solution)/shard_map/dot_general | solution.py:149
  218.3 17.5 %fusion.14 = bf16[256,8,128]{0,2,1:T(8,128)(2,1)S(1)} fusion(bf16[4608,8,128]{0,2,1:T(8,128)(2,1)} %bitcast.67, f32[8,256,4608]{2,1,0:T(8,128)} %get-tuple-element.29, f32[8,256]{1,0:T(8,128)S(1)} %broadcast_maximum_fusion, f32[256,8]{0,1:T(8,128)S(1)} %bitcast.70), kind=kOutput, calls=%fused_computation.18 | convolution fusion | flops 2435317760 | bytes 47726592 | tf_op jit(solution)/shard_map/hqk,khd->hqd/dot_general | solution.py:134
  235.8 2.2 convolution_convert_fusion.2
  238.0 6.8 %reduce-scatter.2.cloned.1.call-done = bf16[128,2048]{1,0:T(8,128)(2,1)} async-done(((bf16[256,2048]{1,0:T(8,128)(2,1)}), bf16[128,2048]{1,0:T(8,128)(2,1)}) %reduce-scatter.2.cloned.1.call-update) | async-done | bytes 524304 | tf_op jit(solution)/shard_map/reduce_scatter | solution.py:154
  244.9 2.0 fusion.22
  (54 shorter events, 1.6 us)
Async XLA Ops:
  6.5 109.3 %copy-start = (bf16[2048,512]{1,0:T(8,128)(2,1)S(1)}, bf16[2048,512]{1,0:T(8,128)(2,1)}, u32[]{:S(2)}) copy-start(bf16[2048,512]{1,0:T(8,128)(2,1)} %param.26) | copy-start | bytes 6291460
  6.5 61.4 %copy-start.6 = (f32[2048]{0:T(1024)S(1)}, f32[2048]{0:T(1024)}, u32[]{:S(2)}) copy-start(f32[2048]{0:T(1024)} %param.24) | copy-start | bytes 24580
  6.5 61.4 %copy-start.5 = (bf16[16,2048]{1,0:T(8,128)(2,1)S(1)}, bf16[16,2048]{1,0:T(8,128)(2,1)}, u32[]{:S(2)}) copy-start(bf16[16,2048]{1,0:T(8,128)(2,1)} %param.20) | copy-start | bytes 196612
  6.5 59.8 %copy-start.4 = (bf16[2048,64]{0,1:T(8,128)(2,1)S(1)}, bf16[2048,64]{0,1:T(8,128)(2,1)}, u32[]{:S(2)}) copy-start(bf16[2048,64]{0,1:T(8,128)(2,1)} %param.28) | copy-start | bytes 786436
  6.5 109.2 %copy-start.7 = (f32[8]{0:T(128)S(1)}, f32[8]{0:T(128)}, u32[]{:S(2)}) copy-start(f32[8]{0:T(128)} %param.32) | copy-start | bytes 100
  6.5 109.3 %all-gather.4.cloned.1.call-start = ((), (), s32[]{:S(2)}) async-start(), calls=%async_computation.1 | async-start | bytes 1572864 | tf_op jit(solution)/shard_map/all_gather | solution.py:107
  58.4 78.0 %all-gather.6.cloned.1.call-start = ((), (), s32[]{:S(2)}) async-start(), calls=%async_computation.2 | async-start | bytes 4866048 | tf_op jit(solution)/shard_map/all_gather | solution.py:145
  66.2 178.6 %reduce-scatter.2.cloned.1.call-start = ((), (), s32[]{:S(2)}) async-start(), calls=%async_computation.3 | async-start | bytes 1572864 | tf_op jit(solution)/shard_map/reduce_scatter | solution.py:154
  145.9 18.4 %copy-start.3 = (bf16[4608,64,1]{0,1,2:T(8,128)(2,1)S(1)}, bf16[4608,64,1]{0,1,2:T(8,128)(2,1)}, u32[]{:S(2)}) copy-start(bf16[4608,64,1]{0,1,2:T(8,128)(2,1)} %reshape.383) | copy-start | bytes 1769476
  192.1 16.3 %copy-start.9 = (bf16[512,1024]{1,0:T(8,128)(2,1)S(1)}, bf16[512,1024]{1,0:T(8,128)(2,1)}, u32[]{:S(2)}) copy-start(bf16[512,1024]{1,0:T(8,128)(2,1)} %param.31) | copy-start | bytes 3145732
  218.2 17.5 %copy-start.8 = (bf16[1024,2048]{1,0:T(8,128)(2,1)S(1)}, bf16[1024,2048]{1,0:T(8,128)(2,1)}, u32[]{:S(2)}) copy-start(bf16[1024,2048]{1,0:T(8,128)(2,1)} %param.33) | copy-start | bytes 12582916
  218.2 26.6 %copy-start.2 = (bf16[128,2048]{1,0:T(8,128)(2,1)S(1)}, bf16[128,2048]{1,0:T(8,128)(2,1)}, u32[]{:S(2)}) copy-start(bf16[128,2048]{1,0:T(8,128)(2,1)} %param.17) | copy-start | bytes 1572868
  218.3 28.6 %copy-start.1 = (bf16[2048,512]{1,0:T(8,128)(2,1)S(1)}, bf16[2048,512]{1,0:T(8,128)(2,1)}, u32[]{:S(2)}) copy-start(bf16[2048,512]{1,0:T(8,128)(2,1)} %param.26) | copy-start | bytes 6291460
Sparse Core Ops, SparseCore 0:
  58.5 8.8 all-gather.3
  70.3 66.0 all-gather.5
  238.1 6.6 reduce-scatter.1
where the time goes:
time: 254 us; the launch traced here: 253 us
  matrix products  102 us (40%)
  blocking collectives  86.6 us (34%)
  other arithmetic  28.2 us (11%)
  waiting for transfers between devices  19.5 us (8%)
  between operations  13.4 us (5%)
  local copies, waits for them, and re-layouts  3.69 us (1%)
    all_gather x1, blocking collectives, body(): lax.all_gather(own_rope, ('sp', 'tp'), axis=0, tiled=True)  44.1 us
    psum x1, blocking collectives, body(): lax.psum((placed[0], placed[1], placed[2]), ('sp', 'tp'))  42.5 us
    dot_general x1, matrix products, fold_keys(): jnp.einsum('qhr,kr->hqk', query_rope, rope_keys, preferred_element_type=j...  27.8 us
    dot_general x1, matrix products, fold_keys(): jnp.einsum('qhd,khd->hqk', query_nope, keys, preferred_element_type=jnp.f...  18.4 us
    dot_general x1, matrix products, fold_keys(): jnp.einsum('hqk,khd->hqd', weights.astype(jnp.bfloat16), values, preferre...  17.5 us
    reduce_sum x1, other arithmetic, fold_keys(): total = jnp.sum(weights, axis=-1)  16.3 us
    all_gather x1, waiting for transfers between devices, body(): lax.all_gather(own_latents, ('sp', 'tp'), axis=0, tiled=True)  12.6 us
    dot_general x1, matrix products, body(): jnp.dot(pieces[0], w_value_up, preferred_element_type=jnp.float32)  9.87 us
  transfers between devices with their start and end apart: 3, of which 2 were waited for; matrix products, arithmetic and copies ran while one was open for 8% of the time, Pallas kernels for 0%

commit v1 on v0

v1 whole, which is shorter than its diff:
```python
import functools

import jax
import jax.numpy as jnp
from jax import lax
from jax.experimental import pallas as pl
from jax.experimental.pallas import tpu as pltpu
from jax.sharding import PartitionSpec as P

GRID_W = 128
EPS = 1e-06
ROPE_BASE = 10000.0
LANES = 128
LOG2E = 1.4426950408889634
FLAGS = 4
MESH = pl.DeviceIdType.MESH
F32 = jnp.float32
BF16 = jnp.bfloat16


def remote(src, dst, send, recv, device):
    return pltpu.make_async_remote_copy(
        src_ref=src, dst_ref=dst, send_sem=send, recv_sem=recv, device_id=device, device_id_type=MESH
    )


def rotate(values, cosine, sine):
    width = values.shape[-1]
    ahead = pltpu.roll(values, width - 1, 1)
    behind = pltpu.roll(values, 1, 1)
    even = lax.broadcasted_iota(jnp.int32, values.shape, 1) % 2 == 0
    return values * cosine + jnp.where(even, ahead, behind) * sine


def modulation_kernel(
    n_sp, n_tp, rows, ctx_rows,
    pair_ref, shift_w, scale_w, gate_w, x_ref, gain_ref, down_ref, rope_ref, kv_gain_ref, cos_ref, sin_ref,
    h_ref, packed_ref, gate_ref,
    part, landed, reduced, full, mods, send1, recv1, send2, recv2,
):
    me = lax.axis_index("sp")
    mine = lax.axis_index("tp")
    total = n_sp * n_tp
    flat = me * n_tp + mine
    barrier = pltpu.get_barrier_semaphore()

    def greet(i, _):
        other = lax.rem(flat + i, total)
        pl.semaphore_signal(barrier, inc=1, device_id=(other // n_tp, other % n_tp), device_id_type=MESH)
        return 0

    lax.fori_loop(1, total, greet, 0)

    columns = shift_w.shape[1]
    blocks = columns // LANES
    per = -(-6 * blocks // n_sp)
    part[...] = jnp.zeros_like(part)
    pair = pair_ref[...]
    for which, weight in enumerate((shift_w, scale_w, gate_w)):
        product = jnp.dot(pair, weight[...], precision=lax.Precision.HIGHEST, preferred_element_type=F32)
        for row in range(2):
            for block in range(blocks):
                unit = (which * 2 + row) * blocks + block
                part[unit // per, unit % per : unit % per + 1, :] = product[
                    row : row + 1, block * LANES : (block + 1) * LANES
                ]
    pl.semaphore_wait(barrier, total - 1)

    def scatter(i, _):
        other = lax.rem(me + i, n_sp)
        remote(part.at[other], landed.at[me], send1.at[other], recv1.at[me], (other, mine)).start()
        return 0

    lax.fori_loop(1, n_sp, scatter, 0)
    landed[me] = part[me]

    def scattered(i, _):
        other = lax.rem(me + i, n_sp)
        remote(part.at[other], landed.at[other], send1.at[other], recv1.at[other], (other, mine)).wait()
        return 0

    lax.fori_loop(1, n_sp, scattered, 0)
    reduced[...] = jnp.sum(landed[...], axis=0)

    def gather(i, _):
        other = lax.rem(flat + i, total)
        remote(
            reduced, full.at[flat], send2.at[other], recv2.at[flat], (other // n_tp, other % n_tp)
        ).start()
        return 0

    lax.fori_loop(1, total, gather, 0)
    full[flat] = reduced[...]
    x = x_ref[...].astype(F32)
    normed = x * lax.rsqrt(jnp.mean(x * x, axis=-1, keepdims=True) + EPS) * gain_ref[...]

    def gathered(i, _):
        other = lax.rem(flat + i, total)
        remote(
            reduced, full.at[other], send2.at[other], recv2.at[other], (other // n_tp, other % n_tp)
        ).wait()
        return 0

    lax.fori_loop(1, total, gathered, 0)
    for unit in range(6 * blocks):
        row, block = unit // blocks, unit % blocks
        for t in range(n_tp):
            at = t * columns + block * LANES
            mods[row : row + 1, at : at + LANES] = full[(unit // per) * n_tp + t, unit % per : unit % per + 1, :]
    index = lax.broadcasted_iota(jnp.int32, (x.shape[0], 1), 0)
    latent_row = index < rows
    shift = jnp.where(latent_row, mods[0:1, :], mods[1:2, :])
    scale = jnp.where(latent_row, mods[2:3, :], mods[3:4, :])
    h = (normed * (1.0 + scale) + shift).astype(BF16)
    gate_ref[...] = mods[4:5, :]
    h_ref[...] = h[:rows]
    inner = jnp.dot(h, down_ref[...], preferred_element_type=F32)
    inner = inner * lax.rsqrt(jnp.mean(inner * inner, axis=-1, keepdims=True) + EPS)
    rank = inner.shape[1]
    packed_ref[:, :rank] = (inner * kv_gain_ref[...]).astype(BF16)
    rope = rope_ref.shape[1]
    key = jnp.dot(h, rope_ref[...], preferred_element_type=F32)
    key = jnp.concatenate([key, jnp.zeros((key.shape[0], LANES - rope), F32)], axis=1)
    key = rotate(key, cos_ref[...], sin_ref[...])
    lane = lax.broadcasted_iota(jnp.int32, key.shape, 1)
    is_ctx = (index >= rows) & (index < rows + ctx_rows)
    is_pad = index >= rows + ctx_rows
    flag = jnp.where(lane < rope + FLAGS - 1, is_ctx.astype(F32), is_pad.astype(F32))
    key = jnp.where(lane < rope, key, jnp.where(lane < rope + FLAGS, flag, 0.0))
    packed_ref[:, rank:] = key.astype(BF16)


def attention_kernel(
    n_sp, n_tp, heads, nope, rope, factor,
    h_ref, packed_ref, bias_ref, cos_ref, sin_ref, qn_ref, qr_ref, ku_ref, vu_ref, wo_ref, latent_ref, gate_ref,
    out_ref,
    buf, hbuf, q, acc, top, total, att, outbox, inbox, send, recv, send_t, recv_t, send_h, recv_h, send_o, recv_o,
):
    me = lax.axis_index("sp")
    mine = lax.axis_index("tp")
    nz = n_sp // 4
    z, side = me // 4, me % 4
    y, x = side // 2, side % 2
    odd = mine % 2
    flip_x = y * 2 + (1 - x)
    flip_y = (1 - y) * 2 + x
    side_a = flip_x * (1 - odd) + flip_y * odd
    side_b = flip_y * (1 - odd) + flip_x * odd
    side_ab = 3 - side
    rows = h_ref.shape[0]
    period, width = packed_ref.shape
    rank = ku_ref.shape[0]

    def column_of(step, t):
        return lax.rem(z + step * (1 - 2 * (t % 2)) + 2 * nz, nz)

    def column(step):
        return column_of(step, mine)

    def peer(zz, ss):
        return (zz * 4 + ss, mine)

    ahead, back = peer(column(1), side), peer(column(-1), side)
    to_a, to_b = peer(z, side_a), peer(z, side_b)
    partners = [lax.rem(mine + i, n_tp) for i in range(1, n_tp)]

    barrier = pltpu.get_barrier_semaphore()
    for other in [ahead, back, to_a, to_b] + [(me, t) for t in partners]:
        pl.semaphore_signal(barrier, inc=1, device_id=other, device_id_type=MESH)
    pl.semaphore_wait(barrier, 3 + n_tp)

    def slot(zz, ss, t):
        return buf.at[t, zz, pl.ds(pl.multiple_of(ss * period, period), period)]

    started = []

    def push(zz, ss, way, device):
        src = packed_ref if way[1] else slot(zz, ss, mine)
        copy = remote(src, slot(zz, ss, mine), send.at[way[0], zz, ss], recv.at[zz, ss], device)
        copy.start()
        started.append(copy)

    def across(zz, ss, own=False):
        src = packed_ref if own else slot(zz, ss, mine)
        for t in partners:
            copy = remote(src, slot(zz, ss, mine), send_t.at[t, zz, ss], recv_t.at[mine, zz, ss], (me, t))
            copy.start()
            started.append(copy)

    def arrived(zz, ss):
        remote(slot(zz, ss, mine), slot(zz, ss, mine), send.at[0, zz, ss], recv.at[zz, ss], ahead).wait_recv()

    forward = nz // 2
    backward = nz - 1 - forward
    order = [0]
    for j in range(1, forward + 1):
        order.append(-j)
        if j <= backward:
            order.append(j)

    for t in partners:
        copy = remote(h_ref, hbuf.at[mine], send_h.at[t], recv_h.at[mine], (me, t))
        copy.start()
        started.append(copy)

    def event_z(step):
        zz = column(step)
        own = step == 0
        if not own:
            arrived(zz, side)
        if own or (step < 0 and -step < forward):
            push(zz, side, (0, own), ahead)
        if own or (step > 0 and step < backward):
            push(zz, side, (1, own), back)
        push(zz, side, (2, own), to_a)
        push(zz, side, (3, own), to_b)
        across(zz, side, own)

    def event_a(step):
        zz = column(step)
        arrived(zz, side_a)
        push(zz, side_a, (3, False), to_b)
        across(zz, side_a)

    def event_b(step, which):
        zz = column(step)
        arrived(zz, which)
        across(zz, which)

    def ready(step):
        for t in partners:
            zz = column_of(step, t)
            for ss in (side, side_a, side_b, side_ab):
                remote(slot(zz, ss, t), slot(zz, ss, t), send_t.at[t, zz, ss], recv_t.at[t, zz, ss], (me, t)).wait_recv()

    event_z(0)
    hbuf[mine] = h_ref[...]
    buf[mine, z, pl.ds(pl.multiple_of(side * period, period), period), :] = packed_ref[...]
    acc[...] = jnp.zeros_like(acc)
    top[...] = jnp.full(top.shape, -1e38, F32)
    total[...] = jnp.zeros_like(total)
    for t in partners:
        remote(h_ref, hbuf.at[t], send_h.at[t], recv_h.at[t], (me, t)).wait_recv()

    tokens = n_tp * rows
    piece = hbuf[...].reshape(tokens, hbuf.shape[2])
    turned = jnp.dot(piece, qr_ref[...], preferred_element_type=F32)
    copies = turned.shape[1] // LANES
    turned = rotate(
        turned, jnp.concatenate([cos_ref[...]] * copies, axis=1), jnp.concatenate([sin_ref[...]] * copies, axis=1)
    ).astype(BF16)
    for head in range(heads):
        q[head, :, :nope] = jnp.dot(
            piece, qn_ref[:, head * nope : (head + 1) * nope], preferred_element_type=F32
        ).astype(BF16)
        q[head, :, nope : nope + rope] = turned[:, head * rope : (head + 1) * rope]
        q[head, :, nope + rope :] = jnp.broadcast_to(
            bias_ref[head : head + 1, :], (tokens, LANES - rope)
        )

    def attend(step):
        places = [(t, column_of(step, t)) for t in range(n_tp)]

        def one(head, _):
            at = pl.ds(pl.multiple_of(head * nope, nope), nope)
            weight = jnp.concatenate([ku_ref[:, at], vu_ref[:, at]], axis=1)
            latents = jnp.concatenate([buf[t, zz, :, :rank] for t, zz in places], axis=0)
            extra = jnp.concatenate([buf[t, zz, :, rank:] for t, zz in places], axis=0)
            both = jnp.dot(latents, weight, preferred_element_type=F32).astype(BF16)
            keys = jnp.concatenate([both[:, :nope], extra], axis=1)
            scores = lax.dot_general(q[head], keys, (((1,), (1,)), ((), ())), preferred_element_type=F32)
            old = top[head][:, :1]
            new = jnp.maximum(old, jnp.max(scores, axis=-1, keepdims=True))
            weights = jnp.exp2((scores - new) * (factor * LOG2E))
            fade = jnp.exp2((old - new) * (factor * LOG2E))
            top[head] = jnp.broadcast_to(new, top.shape[1:])
            total[head] = total[head] * fade + jnp.sum(weights, axis=-1, keepdims=True)
            acc[head] = acc[head] * fade + jnp.dot(
                weights.astype(BF16), both[:, nope:], preferred_element_type=F32
            )
            return 0

        lax.fori_loop(0, heads, one, 0, unroll=min(2, heads))

    def events(step):
        event_z(step)
        event_a(step)
        event_b(step, side_b)
        event_b(step, side_ab)

    event_a(0)
    event_b(0, side_b)
    event_b(0, side_ab)
    ready(0)
    for i, step in enumerate(order):
        if i + 1 < len(order):
            event_z(order[i + 1])
        attend(step)
        if i + 1 < len(order):
            event_a(order[i + 1])
            event_b(order[i + 1], side_b)
            event_b(order[i + 1], side_ab)
            ready(order[i + 1])

    for head in range(heads):
        att[:, head * nope : (head + 1) * nope] = (acc[head] / total[head]).astype(BF16)

    for t in partners:
        lines = pl.ds(pl.multiple_of(t * rows, rows), rows)
        outbox[t] = jnp.dot(att[lines, :], wo_ref[...], preferred_element_type=F32).astype(BF16)
        copy = remote(outbox.at[t], inbox.at[mine], send_o.at[t], recv_o.at[mine], (me, t))
        copy.start()
        started.append(copy)
    lines = pl.ds(pl.multiple_of(mine * rows, rows), rows)
    branch = jnp.dot(att[lines, :], wo_ref[...], preferred_element_type=F32).astype(BF16).astype(F32)
    for t in partners:
        remote(outbox.at[t], inbox.at[t], send_o.at[t], recv_o.at[t], (me, t)).wait_recv()
        branch = branch + inbox[t].astype(F32)
    out_ref[...] = (latent_ref[...].astype(F32) + gate_ref[...] * branch).astype(BF16)
    for copy in started:
        copy.wait_send()


def tables(positions, rope, real):
    quarter = rope // 4
    lane = jnp.arange(LANES, dtype=jnp.int32)
    pair = (lane % rope) // 2
    inverse = ROPE_BASE ** (-(pair % quarter).astype(F32) / quarter)
    place = jnp.where(pair[None, :] < quarter, (positions // GRID_W)[:, None], (positions % GRID_W)[:, None])
    angle = jnp.where(real[:, None], place.astype(F32) * inverse[None, :], 0.0)
    sine = jnp.sin(angle)
    return jnp.cos(angle), jnp.where(lane[None, :] % 2 == 0, -sine, sine)


def body(
    latent, cond, ctx_mod, context, shift_w, scale_w, gate_w, norm_gain, w_qn, w_qr, w_kv_down, w_rope_key,
    kv_gain, w_key_up, w_value_up, ctx_bias, w_out,
):
    n_sp, n_tp = lax.axis_size("sp"), lax.axis_size("tp")
    sp_index, tp_index = lax.axis_index("sp"), lax.axis_index("tp")
    rows, width = latent.shape
    ctx_rows = context.shape[0]
    tokens = rows * n_tp
    heads = ctx_bias.shape[0]
    nope = w_key_up.shape[1] // heads
    rope = w_rope_key.shape[1]
    rank = w_kv_down.shape[1]
    period = -(-(rows + ctx_rows) // 16) * 16
    factor = (nope + rope) ** (-0.5)
    feat = shift_w.shape[0]
    pair = jnp.stack([jax.nn.silu(cond), jax.nn.silu(ctx_mod)])
    pair = lax.dynamic_slice_in_dim(pair, sp_index * feat, feat, 1)
    pair = jnp.concatenate([pair, jnp.zeros((6, feat), F32)], axis=0)
    pad = jnp.zeros((period - rows - ctx_rows, width), BF16)
    x = jnp.concatenate([latent, context, pad], axis=0)
    line = jnp.arange(period, dtype=jnp.int32)
    own_cos, own_sin = tables(sp_index * tokens + tp_index * rows + line, rope, line < rows)
    place = jnp.arange(tokens, dtype=jnp.int32)
    cosine, sine = tables(sp_index * tokens + place, rope, place >= 0)

    vmem = pl.BlockSpec(memory_space=pltpu.VMEM)
    dma = pltpu.SemaphoreType.DMA
    h, packed, gate = pl.pallas_call(
        functools.partial(modulation_kernel, n_sp, n_tp, rows, ctx_rows),
        out_shape=(
            jax.ShapeDtypeStruct((rows, width), BF16),
            jax.ShapeDtypeStruct((period, rank + LANES), BF16),
            jax.ShapeDtypeStruct((1, width), F32),
        ),
        in_specs=[vmem] * 11,
        out_specs=(vmem,) * 3,
        scratch_shapes=[
            pltpu.VMEM((n_sp, 8, LANES), F32),
            pltpu.VMEM((n_sp, 8, LANES), F32),
            pltpu.VMEM((8, LANES), F32),
            pltpu.VMEM((n_sp * n_tp, 8, LANES), F32),
            pltpu.VMEM((8, width), F32),
            dma((n_sp,)),
            dma((n_sp,)),
            dma((n_sp * n_tp,)),
            dma((n_sp * n_tp,)),
        ],
        compiler_params=pltpu.CompilerParams(
            collective_id=0, has_side_effects=True, vmem_limit_bytes=40 * 1024 * 1024
        ),
        name="modulation",
    )(
        pair, shift_w, scale_w, gate_w, x, norm_gain[None, :], w_kv_down, w_rope_key, kv_gain[None, :],
        own_cos, own_sin,
    )

    scaled = ctx_bias / factor
    high = lax.reduce_precision(scaled, 8, 7)
    middle = lax.reduce_precision(scaled - high, 8, 7)
    low = scaled - high - middle
    bias = jnp.stack([high, middle, low, jnp.full_like(scaled, -1e30)], axis=1)
    bias = jnp.concatenate([bias, jnp.zeros((heads, LANES - rope - FLAGS), F32)], axis=1).astype(BF16)
    short = -(heads * rope) % LANES
    if short:
        w_qr = jnp.concatenate([w_qr, jnp.zeros((width, short), BF16)], axis=1)

    nz = n_sp // 4
    return pl.pallas_call(
        functools.partial(attention_kernel, n_sp, n_tp, heads, nope, rope, factor),
        out_shape=jax.ShapeDtypeStruct((rows, width), BF16),
        in_specs=[vmem] * 12,
        out_specs=vmem,
        scratch_shapes=[
            pltpu.VMEM((n_tp, nz, 4 * period, rank + LANES), BF16),
            pltpu.VMEM((n_tp, rows, width), BF16),
            pltpu.VMEM((heads, tokens, nope + LANES), BF16),
            pltpu.VMEM((heads, tokens, nope), F32),
            pltpu.VMEM((heads, tokens, LANES), F32),
            pltpu.VMEM((heads, tokens, LANES), F32),
            pltpu.VMEM((tokens, heads * nope), BF16),
            pltpu.VMEM((n_tp, rows, width), BF16),
            pltpu.VMEM((n_tp, rows, width), BF16),
            dma((4, nz, 4)),
            dma((nz, 4)),
            dma((n_tp, nz, 4)),
            dma((n_tp, nz, 4)),
            dma((n_tp,)),
            dma((n_tp,)),
            dma((n_tp,)),
            dma((n_tp,)),
        ],
        compiler_params=pltpu.CompilerParams(
            collective_id=1, has_side_effects=True, vmem_limit_bytes=60 * 1024 * 1024
        ),
        name="attention",
    )(h, packed, bias, cosine, sine, w_qn, w_qr, w_key_up, w_value_up, w_out, latent, gate)


def solution(mesh):
    placed = (
        P(("sp", "tp"), None),
        P(),
        P(),
        P(("sp", "tp"), None),
        P("sp", "tp"),
        P("sp", "tp"),
        P("sp", "tp"),
        P(),
        P(None, "tp"),
        P(None, "tp"),
        P(),
        P(),
        P(),
        P(None, "tp"),
        P(None, "tp"),
        P("tp"),
        P("tp", None),
    )
    return jax.shard_map(
        body, mesh=mesh, in_specs=placed, out_specs=P(("sp", "tp"), None), check_vma=False
    )
```

time: 254 us -> 116 us (0.46)
  matrix products: 102 us -> 0 us
  Pallas kernels: 0 us -> 102 us
  blocking collectives: 86.6 us -> 0 us
  other arithmetic: 28.2 us -> 4.55 us
  waiting for transfers between devices: 19.5 us -> 0 us
  between operations: 13.4 us -> 0.11 us
  local copies, waits for them, and re-layouts: 3.69 us -> 9.3 us
    pallas_call x0 -> x2, Pallas kernels: none -> 102 us  [the longest x1 84 us: body(): pl.pallas_call(functools.partial(attention_kernel, n_sp, n_tp, heads, nop...]
    dot_general x15 -> x0, matrix products: 102 us -> none  [the longest x1 27.8 us: fold_keys(): jnp.einsum('qhr,kr->hqk', query_rope, rope_keys, preferred_element_type=j...]
    all_gather x1 -> x0, blocking collectives: 44.1 us -> none  [body(): lax.all_gather(own_rope, ('sp', 'tp'), axis=0, tiled=True)]
    psum x1 -> x0, blocking collectives: 42.5 us -> none  [body(): lax.psum((placed[0], placed[1], placed[2]), ('sp', 'tp'))]
    reduce_sum x3 -> x0, other arithmetic: 18.5 us -> none  [the longest x1 16.3 us: fold_keys(): total = jnp.sum(weights, axis=-1)]
    all_gather x2 -> x0, waiting for transfers between devices: 12.6 us -> none  [the longest x1 12.6 us: body(): lax.all_gather(own_latents, ('sp', 'tp'), axis=0, tiled=True)]
    reduce_scatter x1 -> x0, waiting for transfers between devices: 6.83 us -> none  [body(): lax.psum_scatter(jnp.dot(part, w_out, preferred_element_type=jnp.float32)...]
    unnamed x21 -> x22, local copies, waits for them, and re-layouts: 2.52 us -> 8.33 us
  transfers between devices with their start and end apart: 3 -> 0, of which waited for: 2 -> 0; matrix products, arithmetic and copies ran while one was open for 8% -> 0% of each run, Pallas kernels for 0% -> 0%
where the time goes in v1:
time: 116 us
  Pallas kernels  102 us (88%)
  local copies, waits for them, and re-layouts  9.3 us (8%)
  other arithmetic  4.55 us (4%)
    pallas_call x1, Pallas kernels, body(): pl.pallas_call(functools.partial(attention_kernel, n_sp, n_tp, heads, nop...  84 us
    pallas_call x1, Pallas kernels, body(): pl.pallas_call(functools.partial(modulation_kernel, n_sp, n_tp, rows, ctx...  18 us
    unnamed x22, local copies, waits for them, and re-layouts  8.33 us

profile of v1, /device:TPU:0, one launch (start us, length us, event | category | flops | bytes accessed | tf_op | source)
XLA Modules:
  0.0 116.0 jit_solution(14404230280080602896)
XLA Ops:
  0.0 0.0 copy-start.6
  0.0 0.0 copy-start.8
  0.0 0.0 copy-start
  0.1 0.4 negate_select_fusion.1
  0.5 0.9 divide_multiply_fusion.1
  1.4 0.7 divide_multiply_fusion
  2.1 0.1 fusion.2
  2.2 1.1 pad_maximum_fusion.x_ref
  3.3 1.3 %copy.18.rope_ref = bf16[2048,64]{1,0:T(8,128)(2,1)S(1)} copy(bf16[2048,64]{0,1:T(8,128)(2,1)} %param.28) | data formatting | bytes 524288 | tf_op args[11]
  4.6 0.0 copy-done.6
  4.6 0.0 copy-done.8
  4.6 0.0 copy-done
  4.6 0.0 copy-start.2
  4.6 1.0 copy-done.2
  5.7 0.0 copy-start.3
  5.7 1.0 copy-done.3
  6.7 0.0 copy-start.4
  6.7 1.0 copy-done.4
  7.7 0.0 copy-start.9
  7.7 18.0 %modulation.1 = (bf16[128,2048]{1,0:T(8,128)(2,1)S(1)}, bf16[144,640]{1,0:T(8,128)(2,1)S(1)}, f32[1,2048]{1,0:T(1,128)S(1)}) custom-call(f32[8,128]{1,0:T(8,128)S(1)} %concatenate.10.pair_ref, f32[128,1024]{1,0:T(8,128)S(1)} %copy-done.2, f32[128,1024]{1,0:T(8,128)S(1)} %copy-done.3, f32[128,1024]{1,0:T(8,128)S(1)} %copy-done.4, ...), custom_call_target="tpu_custom_call" | custom-call | tf_op jit(solution)/shard_map/modulation/pallas_call | solution.py:363
  25.7 0.0 copy-start.1
  25.8 0.8 copy-done.1
  26.5 0.7 copy-done.5
  27.2 0.6 copy-done.7
  27.8 1.3 %negate_select_fusion = (f32[256,128]{1,0:T(8,128)}, f32[256,128]{1,0:T(8,128)}) fusion(f32[128]{0:T(128)S(1)} %fusion.12, s32[256]{0:T(256)S(1)} %get-tuple-element.20, s32[256]{0:T(256)S(1)} %get-tuple-element.21, pred[128]{0:T(512)(128)(4,1)S(1)} %get-tuple-element.18, pred[128]{0:T(512)(128)(4,1)S(1)} %get-tuple-element.19), kind=kLoop, calls=%fused_computation.1 | loop fusion | flops 163840 | bytes 264960 | tf_op jit(solution)/shard_map/jit(_where)/select_n | solution.py:332
  29.1 0.0 copy-done.9
  29.1 0.1 copy.19
  29.2 0.1 copy.20
  29.3 0.1 copy.21
  29.4 0.7 concatenate.12.bias_ref
  30.1 84.0 %attention.1 = bf16[128,2048]{1,0:T(8,128)(2,1)} custom-call(bf16[128,2048]{1,0:T(8,128)(2,1)} %copy-done.1, bf16[144,640]{1,0:T(8,128)(2,1)} %copy-done.5, bf16[8,64]{1,0:T(8,128)(2,1)} %concatenate.12.bias_ref, f32[256,128]{1,0:T(8,128)} %get-tuple-element.14.cos_ref, f32[256,128]{1,0:T(8,128)} %get-tuple-element.13.sin_ref, bf16[2048,1024]{1,0:T(8,128)(2,1)} %qn_ref.1, ...), custom_call_target="tpu_custom_call" | custom-call | tf_op jit(solution)/shard_map/attention/pallas_call | solution.py:403
  114.1 1.9 %copy.23 = bf16[128,2048]{1,0:T(8,128)(2,1)} copy(bf16[128,2048]{1,0:T(8,128)(2,1)} %attention.1) | data formatting | bytes 1048576
  (11 shorter events, 0.1 us)
Async XLA Ops:
  0.0 4.6 %copy-start.6 = (f32[2048]{0:T(1024)S(1)}, f32[2048]{0:T(1024)}, u32[]{:S(2)}) copy-start(f32[2048]{0:T(1024)} %param.24) | copy-start | bytes 24580
  0.0 4.6 %copy-start.8 = (f32[512]{0:T(512)S(1)}, f32[512]{0:T(512)}, u32[]{:S(2)}) copy-start(f32[512]{0:T(512)} %param.29) | copy-start | bytes 6148
  0.0 4.6 %copy-start = (bf16[2048,512]{1,0:T(8,128)(2,1)S(1)}, bf16[2048,512]{1,0:T(8,128)(2,1)}, u32[]{:S(2)}) copy-start(bf16[2048,512]{1,0:T(8,128)(2,1)} %down_ref.1) | copy-start | bytes 6291460
  4.6 1.0 copy-start.2
  5.7 1.0 copy-start.3
  6.7 1.0 copy-start.4
  7.7 21.3 %copy-start.9 = (f32[8]{0:T(128)S(1)}, f32[8]{0:T(128)}, u32[]{:S(2)}) copy-start(f32[8]{0:T(128)} %param.32) | copy-start | bytes 100
  25.7 0.8 copy-start.1
  26.5 0.7 copy-start.5
  27.2 0.6 copy-start.7

commit v2 on v1

--- a/solution.py
+++ b/solution.py
@@ -132,12 +132,21 @@
 
 def attention_kernel(
     n_sp, n_tp, heads, nope, rope, factor,
-    h_ref, packed_ref, bias_ref, cos_ref, sin_ref, qn_ref, qr_ref, ku_ref, vu_ref, wo_ref, latent_ref, gate_ref,
+    h_ref, packed_ref, bias_ref, cos_ref, sin_ref, qn_hbm, qr_hbm, ku_hbm, vu_hbm, wo_hbm, latent_ref, gate_ref,
     out_ref,
+    qr_ref, qn_ref, ku_ref, vu_ref, wo_ref, load_sem,
     buf, hbuf, q, acc, top, total, att, outbox, inbox, send, recv, send_t, recv_t, send_h, recv_h, send_o, recv_o,
 ):
     me = lax.axis_index("sp")
     mine = lax.axis_index("tp")
+    loads = [
+        pltpu.make_async_copy(src, dst, load_sem.at[i])
+        for i, (src, dst) in enumerate(
+            ((qr_hbm, qr_ref), (qn_hbm, qn_ref), (ku_hbm, ku_ref), (vu_hbm, vu_ref), (wo_hbm, wo_ref))
+        )
+    ]
+    for load in loads:
+        load.start()
     nz = n_sp // 4
     z, side = me // 4, me % 4
     y, x = side // 2, side % 2
@@ -174,18 +183,24 @@
 
     started = []
 
-    def push(zz, ss, way, device):
-        src = packed_ref if way[1] else slot(zz, ss, mine)
-        copy = remote(src, slot(zz, ss, mine), send.at[way[0], zz, ss], recv.at[zz, ss], device)
-        copy.start()
-        started.append(copy)
-
-    def across(zz, ss, own=False):
+    def link(step, ss, way, own, device):
+        zz = column(step)
         src = packed_ref if own else slot(zz, ss, mine)
+        return remote(src, slot(zz, ss, mine), send.at[way, zz, ss], recv.at[zz, ss], device)
+
+    def over(step, ss, own, t):
+        zz = column(step)
+        src = packed_ref if own else slot(zz, ss, mine)
+        return remote(src, slot(zz, ss, mine), send_t.at[t, zz, ss], recv_t.at[mine, zz, ss], (me, t))
+
+    def push(step, ss, way, own, device):
+        link(step, ss, way, own, device).start()
+        started.append(lambda: link(step, ss, way, own, device))
+
+    def across(step, ss, own=False):
         for t in partners:
-            copy = remote(src, slot(zz, ss, mine), send_t.at[t, zz, ss], recv_t.at[mine, zz, ss], (me, t))
-            copy.start()
-            started.append(copy)
+            over(step, ss, own, t).start()
+            started.append(lambda t=t: over(step, ss, own, t))
 
     def arrived(zz, ss):
         remote(slot(zz, ss, mine), slot(zz, ss, mine), send.at[0, zz, ss], recv.at[zz, ss], ahead).wait_recv()
@@ -201,7 +216,7 @@
     for t in partners:
         copy = remote(h_ref, hbuf.at[mine], send_h.at[t], recv_h.at[mine], (me, t))
         copy.start()
-        started.append(copy)
+        started.append(lambda copy=copy: copy)
 
     def event_z(step):
         zz = column(step)
@@ -209,23 +224,23 @@
         if not own:
             arrived(zz, side)
         if own or (step < 0 and -step < forward):
-            push(zz, side, (0, own), ahead)
+            push(step, side, 0, own, ahead)
         if own or (step > 0 and step < backward):
-            push(zz, side, (1, own), back)
-        push(zz, side, (2, own), to_a)
-        push(zz, side, (3, own), to_b)
-        across(zz, side, own)
+            push(step, side, 1, own, back)
+        push(step, side, 2, own, to_a)
+        push(step, side, 3, own, to_b)
+        across(step, side, own)
 
     def event_a(step):
         zz = column(step)
         arrived(zz, side_a)
-        push(zz, side_a, (3, False), to_b)
-        across(zz, side_a)
+        push(step, side_a, 3, False, to_b)
+        across(step, side_a)
 
     def event_b(step, which):
         zz = column(step)
         arrived(zz, which)
-        across(zz, which)
+        across(step, which)
 
     def ready(step):
         for t in partners:
@@ -244,11 +259,13 @@
 
     tokens = n_tp * rows
     piece = hbuf[...].reshape(tokens, hbuf.shape[2])
+    loads[0].wait()
     turned = jnp.dot(piece, qr_ref[...], preferred_element_type=F32)
     copies = turned.shape[1] // LANES
     turned = rotate(
         turned, jnp.concatenate([cos_ref[...]] * copies, axis=1), jnp.concatenate([sin_ref[...]] * copies, axis=1)
     ).astype(BF16)
+    loads[1].wait()
     for head in range(heads):
         q[head, :, :nope] = jnp.dot(
             piece, qn_ref[:, head * nope : (head + 1) * nope], preferred_element_type=F32
@@ -258,7 +275,7 @@
             bias_ref[head : head + 1, :], (tokens, LANES - rope)
         )
 
-    def attend(step):
+    def attend(step, beside):
         places = [(t, column_of(step, t)) for t in range(n_tp)]
 
         def one(head, _):
@@ -280,27 +297,42 @@
             )
             return 0
 
-        lax.fori_loop(0, heads, one, 0, unroll=min(2, heads))
-
-    def events(step):
-        event_z(step)
-        event_a(step)
-        event_b(step, side_b)
-        event_b(step, side_ab)
+        together = 2 if heads % 2 == 0 else 1
+
+        def some(i, _):
+            for k, event in enumerate(beside):
+                if k < heads // together:
+                    pl.when(i == k)(event)
+            for j in range(together):
+                one(i * together + j, 0)
+            return 0
+
+        lax.fori_loop(0, heads // together, some, 0)
+        for event in beside[heads // together :]:
+            event()
 
     event_a(0)
     event_b(0, side_b)
     event_b(0, side_ab)
     ready(0)
+    loads[2].wait()
+    loads[3].wait()
     for i, step in enumerate(order):
         if i + 1 < len(order):
-            event_z(order[i + 1])
-        attend(step)
-        if i + 1 < len(order):
-            event_a(order[i + 1])
-            event_b(order[i + 1], side_b)
-            event_b(order[i + 1], side_ab)
-            ready(order[i + 1])
+            later = order[i + 1]
+            attend(
+                step,
+                [
+                    functools.partial(event_z, later),
+                    functools.partial(event_a, later),
+                    functools.partial(event_b, later, side_b),
+                    functools.partial(event_b, later, side_ab),
+                ],
+            )
+            ready(later)
+        else:
+            attend(step, [])
+    loads[4].wait()
 
     for head in range(heads):
         att[:, head * nope : (head + 1) * nope] = (acc[head] / total[head]).astype(BF16)
@@ -310,15 +342,15 @@
         outbox[t] = jnp.dot(att[lines, :], wo_ref[...], preferred_element_type=F32).astype(BF16)
         copy = remote(outbox.at[t], inbox.at[mine], send_o.at[t], recv_o.at[mine], (me, t))
         copy.start()
-        started.append(copy)
+        started.append(lambda copy=copy: copy)
     lines = pl.ds(pl.multiple_of(mine * rows, rows), rows)
     branch = jnp.dot(att[lines, :], wo_ref[...], preferred_element_type=F32).astype(BF16).astype(F32)
     for t in partners:
         remote(outbox.at[t], inbox.at[t], send_o.at[t], recv_o.at[t], (me, t)).wait_recv()
         branch = branch + inbox[t].astype(F32)
     out_ref[...] = (latent_ref[...].astype(F32) + gate_ref[...] * branch).astype(BF16)
-    for copy in started:
-        copy.wait_send()
+    for make in started:
+        make().wait_send()
 
 
 def tables(positions, rope, real):
@@ -403,9 +435,15 @@
     return pl.pallas_call(
         functools.partial(attention_kernel, n_sp, n_tp, heads, nope, rope, factor),
         out_shape=jax.ShapeDtypeStruct((rows, width), BF16),
-        in_specs=[vmem] * 12,
+        in_specs=[vmem] * 5 + [pl.BlockSpec(memory_space=pl.ANY)] * 5 + [vmem] * 2,
         out_specs=vmem,
         scratch_shapes=[
+            pltpu.VMEM(w_qr.shape, BF16),
+            pltpu.VMEM(w_qn.shape, BF16),
+            pltpu.VMEM(w_key_up.shape, BF16),
+            pltpu.VMEM(w_value_up.shape, BF16),
+            pltpu.VMEM(w_out.shape, BF16),
+            dma((5,)),
             pltpu.VMEM((n_tp, nz, 4 * period, rank + LANES), BF16),
             pltpu.VMEM((n_tp, rows, width), BF16),
             pltpu.VMEM((heads, tokens, nope + LANES), BF16),

time: 116 us -> 106 us (0.914)
  Pallas kernels: 102 us -> 91.4 us
    pallas_call x1, Pallas kernels: 84 us -> 73.4 us  [body(): pl.pallas_call(functools.partial(attention_kernel, n_sp, n_tp, heads, nop...]
where the time goes in v2:
time: 106 us; the launch traced here: 105 us
  Pallas kernels  91.4 us (86%)
  local copies, waits for them, and re-layouts  9.3 us (9%)
  other arithmetic  4.55 us (4%)
    pallas_call x1, Pallas kernels, body(): pl.pallas_call(functools.partial(attention_kernel, n_sp, n_tp, heads, nop...  73.4 us
    pallas_call x1, Pallas kernels, body(): pl.pallas_call(functools.partial(modulation_kernel, n_sp, n_tp, rows, ctx...  18 us
    unnamed x22, local copies, waits for them, and re-layouts  8.33 us

profile of v2, /device:TPU:0, one launch (start us, length us, event | category | flops | bytes accessed | tf_op | source)
XLA Modules:
  0.0 105.4 jit_solution(12991856259943212449)
XLA Ops:
  0.0 0.0 copy-start.6
  0.0 0.0 copy-start.8
  0.0 0.0 copy-start
  0.1 0.4 negate_select_fusion.1
  0.5 0.9 divide_multiply_fusion.1
  1.4 0.7 divide_multiply_fusion
  2.1 0.1 fusion.2
  2.2 1.1 %pad_maximum_fusion.x_ref = bf16[144,2048]{1,0:T(8,128)(2,1)S(1)} fusion(bf16[16,2048]{1,0:T(8,128)(2,1)} %param.20, bf16[128,2048]{1,0:T(8,128)(2,1)} %latent_ref.1), kind=kLoop, calls=%fused_computation | loop fusion | flops 1179648 | bytes 1179648 | tf_op jit(solution)/shard_map/concatenate | solution.py:387
  3.3 1.3 %copy.18.rope_ref = bf16[2048,64]{1,0:T(8,128)(2,1)S(1)} copy(bf16[2048,64]{0,1:T(8,128)(2,1)} %param.28) | data formatting | bytes 524288 | tf_op args[11]
  4.6 0.0 copy-done.6
  4.6 0.0 copy-done.8
  4.6 0.0 copy-done
  4.6 0.0 copy-start.2
  4.6 1.0 copy-done.2
  5.7 0.0 copy-start.3
  5.7 1.0 copy-done.3
  6.7 0.0 copy-start.4
  6.7 1.0 copy-done.4
  7.7 0.0 copy-start.9
  7.7 18.0 %modulation.1 = (bf16[128,2048]{1,0:T(8,128)(2,1)S(1)}, bf16[144,640]{1,0:T(8,128)(2,1)S(1)}, f32[1,2048]{1,0:T(1,128)S(1)}) custom-call(f32[8,128]{1,0:T(8,128)S(1)} %concatenate.10.pair_ref, f32[128,1024]{1,0:T(8,128)S(1)} %copy-done.2, f32[128,1024]{1,0:T(8,128)S(1)} %copy-done.3, f32[128,1024]{1,0:T(8,128)S(1)} %copy-done.4, ...), custom_call_target="tpu_custom_call" | custom-call | tf_op jit(solution)/shard_map/modulation/pallas_call | solution.py:395
  25.7 0.0 copy-start.1
  25.8 0.8 copy-done.1
  26.5 0.7 copy-done.5
  27.2 0.6 copy-done.7
  27.8 1.3 %negate_select_fusion = (f32[256,128]{1,0:T(8,128)}, f32[256,128]{1,0:T(8,128)}) fusion(f32[128]{0:T(128)S(1)} %fusion.12, s32[256]{0:T(256)S(1)} %get-tuple-element.20, s32[256]{0:T(256)S(1)} %get-tuple-element.21, pred[128]{0:T(512)(128)(4,1)S(1)} %get-tuple-element.18, pred[128]{0:T(512)(128)(4,1)S(1)} %get-tuple-element.19), kind=kLoop, calls=%fused_computation.1 | loop fusion | flops 163840 | bytes 264960 | tf_op jit(solution)/shard_map/jit(_where)/select_n | solution.py:364
  29.1 0.0 copy-done.9
  29.1 0.1 copy.19
  29.2 0.1 copy.20
  29.3 0.1 copy.21
  29.4 0.7 concatenate.12.bias_ref
  30.1 73.4 %attention.1 = bf16[128,2048]{1,0:T(8,128)(2,1)} custom-call(bf16[128,2048]{1,0:T(8,128)(2,1)} %copy-done.1, bf16[144,640]{1,0:T(8,128)(2,1)} %copy-done.5, bf16[8,64]{1,0:T(8,128)(2,1)} %concatenate.12.bias_ref, f32[256,128]{1,0:T(8,128)} %get-tuple-element.14.cos_ref, f32[256,128]{1,0:T(8,128)} %get-tuple-element.13.sin_ref, bf16[2048,1024]{1,0:T(8,128)(2,1)} %qn_hbm.1, ...), custom_call_target="tpu_custom_call" | custom-call | tf_op jit(solution)/shard_map/attention/pallas_call | solution.py:435
  103.5 1.9 %copy.23 = bf16[128,2048]{1,0:T(8,128)(2,1)} copy(bf16[128,2048]{1,0:T(8,128)(2,1)} %attention.1) | data formatting | bytes 1048576
  (11 shorter events, 0.1 us)
Async XLA Ops:
  0.0 4.6 %copy-start.6 = (f32[2048]{0:T(1024)S(1)}, f32[2048]{0:T(1024)}, u32[]{:S(2)}) copy-start(f32[2048]{0:T(1024)} %param.24) | copy-start | bytes 24580
  0.0 4.6 %copy-start.8 = (f32[512]{0:T(512)S(1)}, f32[512]{0:T(512)}, u32[]{:S(2)}) copy-start(f32[512]{0:T(512)} %param.29) | copy-start | bytes 6148
  0.0 4.6 %copy-start = (bf16[2048,512]{1,0:T(8,128)(2,1)S(1)}, bf16[2048,512]{1,0:T(8,128)(2,1)}, u32[]{:S(2)}) copy-start(bf16[2048,512]{1,0:T(8,128)(2,1)} %down_ref.1) | copy-start | bytes 6291460
  4.6 1.0 copy-start.2
  5.7 1.0 copy-start.3
  6.7 1.0 copy-start.4
  7.7 21.3 %copy-start.9 = (f32[8]{0:T(128)S(1)}, f32[8]{0:T(128)}, u32[]{:S(2)}) copy-start(f32[8]{0:T(128)} %param.32) | copy-start | bytes 100
  25.7 0.8 copy-start.1
  26.5 0.7 copy-start.5
  27.2 0.6 copy-start.7

commit v3 on v2

--- a/solution.py
+++ b/solution.py
@@ -297,21 +297,20 @@
             )
             return 0
 
-        together = 2 if heads % 2 == 0 else 1
+        together = next(n for n in (4, 2, 1) if heads % n == 0)
+        turns = heads // together
 
         def some(i, _):
             for k, event in enumerate(beside):
-                if k < heads // together:
-                    pl.when(i == k)(event)
+                pl.when(i == k * turns // len(beside))(event)
             for j in range(together):
                 one(i * together + j, 0)
             return 0
 
-        lax.fori_loop(0, heads // together, some, 0)
-        for event in beside[heads // together :]:
-            event()
+        lax.fori_loop(0, turns, some, 0)
 
     event_a(0)
+    event_z(order[1])
     event_b(0, side_b)
     event_b(0, side_ab)
     ready(0)
@@ -323,11 +322,11 @@
             attend(
                 step,
                 [
-                    functools.partial(event_z, later),
                     functools.partial(event_a, later),
                     functools.partial(event_b, later, side_b),
                     functools.partial(event_b, later, side_ab),
-                ],
+                ]
+                + [functools.partial(event_z, step) for step in order[i + 2 : i + 3]],
             )
             ready(later)
         else:

time: 106 us -> 98.2 us (0.926)
  Pallas kernels: 91.4 us -> 83.7 us
    pallas_call x1, Pallas kernels: 73.4 us -> 65.7 us  [body(): pl.pallas_call(functools.partial(attention_kernel, n_sp, n_tp, heads, nop...]
where the time goes in v3:
time: 98.2 us; the launch traced here: 97.7 us
  Pallas kernels  83.7 us (85%)
  local copies, waits for them, and re-layouts  9.3 us (9%)
  other arithmetic  4.55 us (5%)
    pallas_call x1, Pallas kernels, body(): pl.pallas_call(functools.partial(attention_kernel, n_sp, n_tp, heads, nop...  65.7 us
    pallas_call x1, Pallas kernels, body(): pl.pallas_call(functools.partial(modulation_kernel, n_sp, n_tp, rows, ctx...  18 us
    unnamed x22, local copies, waits for them, and re-layouts  8.33 us

profile of v3, /device:TPU:0, one launch (start us, length us, event | category | flops | bytes accessed | tf_op | source)
XLA Modules:
  0.0 97.7 jit_solution(1619178674030687626)
XLA Ops:
  0.0 0.0 copy-start.6
  0.0 0.0 copy-start.8
  0.0 0.0 copy-start
  0.1 0.4 negate_select_fusion.1
  0.5 0.9 divide_multiply_fusion.1
  1.4 0.7 divide_multiply_fusion
  2.1 0.1 fusion.2
  2.2 1.1 %pad_maximum_fusion.x_ref = bf16[144,2048]{1,0:T(8,128)(2,1)S(1)} fusion(bf16[16,2048]{1,0:T(8,128)(2,1)} %param.20, bf16[128,2048]{1,0:T(8,128)(2,1)} %latent_ref.1), kind=kLoop, calls=%fused_computation | loop fusion | flops 1179648 | bytes 1179648 | tf_op jit(solution)/shard_map/concatenate | solution.py:386
  3.3 1.3 %copy.18.rope_ref = bf16[2048,64]{1,0:T(8,128)(2,1)S(1)} copy(bf16[2048,64]{0,1:T(8,128)(2,1)} %param.28) | data formatting | bytes 524288 | tf_op args[11]
  4.6 0.0 copy-done.6
  4.6 0.0 copy-done.8
  4.6 0.0 copy-done
  4.6 0.0 copy-start.2
  4.6 1.0 %copy-done.2 = f32[128,1024]{1,0:T(8,128)S(1)} copy-done((f32[128,1024]{1,0:T(8,128)S(1)}, f32[128,1024]{1,0:T(8,128)}, u32[]{:S(2)}) %copy-start.2) | copy-done | bytes 524312
  5.7 0.0 copy-start.3
  5.7 1.0 %copy-done.3 = f32[128,1024]{1,0:T(8,128)S(1)} copy-done((f32[128,1024]{1,0:T(8,128)S(1)}, f32[128,1024]{1,0:T(8,128)}, u32[]{:S(2)}) %copy-start.3) | copy-done | bytes 524312
  6.7 0.0 copy-start.4
  6.7 1.0 %copy-done.4 = f32[128,1024]{1,0:T(8,128)S(1)} copy-done((f32[128,1024]{1,0:T(8,128)S(1)}, f32[128,1024]{1,0:T(8,128)}, u32[]{:S(2)}) %copy-start.4) | copy-done | bytes 524312
  7.7 0.0 copy-start.9
  7.7 18.0 %modulation.1 = (bf16[128,2048]{1,0:T(8,128)(2,1)S(1)}, bf16[144,640]{1,0:T(8,128)(2,1)S(1)}, f32[1,2048]{1,0:T(1,128)S(1)}) custom-call(f32[8,128]{1,0:T(8,128)S(1)} %concatenate.10.pair_ref, f32[128,1024]{1,0:T(8,128)S(1)} %copy-done.2, f32[128,1024]{1,0:T(8,128)S(1)} %copy-done.3, f32[128,1024]{1,0:T(8,128)S(1)} %copy-done.4, ...), custom_call_target="tpu_custom_call" | custom-call | tf_op jit(solution)/shard_map/modulation/pallas_call | solution.py:394
  25.7 0.0 copy-start.1
  25.8 0.8 copy-done.1
  26.5 0.7 copy-done.5
  27.2 0.6 copy-done.7
  27.8 1.3 %negate_select_fusion = (f32[256,128]{1,0:T(8,128)}, f32[256,128]{1,0:T(8,128)}) fusion(f32[128]{0:T(128)S(1)} %fusion.12, s32[256]{0:T(256)S(1)} %get-tuple-element.20, s32[256]{0:T(256)S(1)} %get-tuple-element.21, pred[128]{0:T(512)(128)(4,1)S(1)} %get-tuple-element.18, pred[128]{0:T(512)(128)(4,1)S(1)} %get-tuple-element.19), kind=kLoop, calls=%fused_computation.1 | loop fusion | flops 163840 | bytes 264960 | tf_op jit(solution)/shard_map/jit(_where)/select_n | solution.py:363
  29.1 0.0 copy-done.9
  29.1 0.1 copy.19
  29.2 0.1 copy.20
  29.3 0.1 copy.21
  29.4 0.7 concatenate.12.bias_ref
  30.1 65.7 %attention.1 = bf16[128,2048]{1,0:T(8,128)(2,1)} custom-call(bf16[128,2048]{1,0:T(8,128)(2,1)} %copy-done.1, bf16[144,640]{1,0:T(8,128)(2,1)} %copy-done.5, bf16[8,64]{1,0:T(8,128)(2,1)} %concatenate.12.bias_ref, f32[256,128]{1,0:T(8,128)} %get-tuple-element.14.cos_ref, f32[256,128]{1,0:T(8,128)} %get-tuple-element.13.sin_ref, bf16[2048,1024]{1,0:T(8,128)(2,1)} %qn_hbm.1, ...), custom_call_target="tpu_custom_call" | custom-call | tf_op jit(solution)/shard_map/attention/pallas_call | solution.py:434
  95.8 1.9 %copy.23 = bf16[128,2048]{1,0:T(8,128)(2,1)} copy(bf16[128,2048]{1,0:T(8,128)(2,1)} %attention.1) | data formatting | bytes 1048576
  (11 shorter events, 0.1 us)
Async XLA Ops:
  0.0 4.6 %copy-start.6 = (f32[2048]{0:T(1024)S(1)}, f32[2048]{0:T(1024)}, u32[]{:S(2)}) copy-start(f32[2048]{0:T(1024)} %param.24) | copy-start | bytes 24580
  0.0 4.6 %copy-start.8 = (f32[512]{0:T(512)S(1)}, f32[512]{0:T(512)}, u32[]{:S(2)}) copy-start(f32[512]{0:T(512)} %param.29) | copy-start | bytes 6148
  0.0 4.6 %copy-start = (bf16[2048,512]{1,0:T(8,128)(2,1)S(1)}, bf16[2048,512]{1,0:T(8,128)(2,1)}, u32[]{:S(2)}) copy-start(bf16[2048,512]{1,0:T(8,128)(2,1)} %down_ref.1) | copy-start | bytes 6291460
  4.6 1.0 %copy-start.2 = (f32[128,1024]{1,0:T(8,128)S(1)}, f32[128,1024]{1,0:T(8,128)}, u32[]{:S(2)}) copy-start(f32[128,1024]{1,0:T(8,128)} %shift_w.1) | copy-start | bytes 1572868
  5.7 1.0 %copy-start.3 = (f32[128,1024]{1,0:T(8,128)S(1)}, f32[128,1024]{1,0:T(8,128)}, u32[]{:S(2)}) copy-start(f32[128,1024]{1,0:T(8,128)} %scale_w.1) | copy-start | bytes 1572868
  6.7 1.0 %copy-start.4 = (f32[128,1024]{1,0:T(8,128)S(1)}, f32[128,1024]{1,0:T(8,128)}, u32[]{:S(2)}) copy-start(f32[128,1024]{1,0:T(8,128)} %gate_w.1) | copy-start | bytes 1572868
  7.7 21.3 %copy-start.9 = (f32[8]{0:T(128)S(1)}, f32[8]{0:T(128)}, u32[]{:S(2)}) copy-start(f32[8]{0:T(128)} %param.32) | copy-start | bytes 100
  25.7 0.8 copy-start.1
  26.5 0.7 copy-start.5
  27.2 0.6 copy-start.7
